TPU v7x, 32 devices: a whole 2x2x4 slice. The times are simulated.
32 devices in a mesh: dp: 4 (over y, x), kv: 4 (over z), tp: 2 (over core).
Axes of the slice: x: 2, y: 2, z: 4, core: 2. Of those that a mesh axis runs over, the one named last changes fastest.
Arguments:
- tokens: bfloat16 [16, 16, 2048], P('dp', None, 'kv'), may hold values from -6 to 6
- norm_gain: float32 [2048], P('kv'), may hold values from 0.1 to 1.9
- w_query: bfloat16 [2048, 1024], P('kv', 'tp'), may hold values from -0.125 to 0.125
- w_key: bfloat16 [2048, 1024], P('kv', 'tp'), may hold values from -0.125 to 0.125
- w_value: bfloat16 [2048, 1024], P('kv', 'tp'), may hold values from -0.125 to 0.125
- w_forget: bfloat16 [2048, 16], replicated, may hold values from -0.125 to 0.125
- forget_bias: float32 [16], replicated, may hold values from -2 to 4
- query_gain: float32 [64], replicated, may hold values from 0.1 to 1.9
- key_gain: float32 [64], replicated, may hold values from 0.1 to 1.9
- head_gain: float32 [64], replicated, may hold values from 0.1 to 1.9
- w_out: bfloat16 [1024, 2048], P('tp', 'kv'), may hold values from -0.1875 to 0.1875
- key_cache: bfloat16 [16, 2048, 1024], P('dp', 'kv', 'tp'), may hold values from -240 to 240
- value_cache: bfloat16 [16, 2048, 1024], P('dp', 'kv', 'tp'), may hold values from -6 to 6
- gate_cache: float32 [16, 16, 2048], P('dp', 'tp', 'kv'), may hold values from -242 to 0, as said below
- lengths: int32 [16], P('dp'), may hold values from 1005 to 2028
- accepted: int32 [16], P('dp'), may hold values from 0 to 4
- parents: int32 [16, 16], P('dp'), may hold values from -1 to 14, as said below
Outputs:
- layer_out: bfloat16 [16, 16, 2048], P('dp', None, 'kv')
- new_keys: bfloat16 [16, 2048, 1024], P('dp', 'kv', 'tp')
- new_values: bfloat16 [16, 2048, 1024], P('dp', 'kv', 'tp')
- proposal_gates: float32 [16, 16, 16], P('dp', None, 'tp')
Inputs may be any that keep to these rules, and one draw needn't show every extreme that they name: `gate_cache`: each entry is the running sum of log forget gates up to its position, so entries never rise along positions; entries at and after lengths hold the last step's proposals in order. `parents`: proposal 0 follows the last accepted token (parent -1); every other proposal's parent is one of the three proposals before it.
All inputs are finite; a program needn't handle non-finite values.
Results may differ from a plain program's by a relative error of at most 0.0051.
The roundings to bfloat16 on the way count: a program that leaves them out, or rounds other values in their place, can miss the bound.
Values may be sent and summed in bfloat16 or wider, within the bound.
A program may use at most 64 MiB of HBM per device.

v0:
```python
import jax
import jax.numpy as jnp
from jax import lax
from jax.sharding import PartitionSpec as P

EPSILON = 1e-06
MASKED = -1e30


def head_norm(head_rows, gain_vec):
    mean_square = jnp.mean(head_rows * head_rows, axis=-1, keepdims=True)
    return head_rows * lax.rsqrt(mean_square + EPSILON) * gain_vec


def ancestry(parents):
    count_all = parents.shape[1]
    step_ids = jnp.arange(count_all, dtype=jnp.int32)
    step_matrix = (parents[:, :, None] == step_ids[None, None, :]).astype(jnp.float32)
    identity = jnp.broadcast_to(jnp.eye(count_all, dtype=jnp.float32), step_matrix.shape)

    def extend(turn_index, ancestors):
        return identity + jnp.einsum(
            "sij,sjk->sik", step_matrix, ancestors, precision=lax.Precision.HIGHEST
        )

    return lax.fori_loop(0, count_all, extend, identity)


def combine(earlier, later):
    earlier_max, earlier_total, earlier_sum = earlier
    later_max, later_total, later_sum = later
    row_max = jnp.maximum(earlier_max, later_max)
    earlier_scale = jnp.exp(earlier_max - row_max)
    later_scale = jnp.exp(later_max - row_max)
    spread = earlier_max.shape + (-1,)
    joined = (
        earlier_sum.reshape(spread) * earlier_scale[..., None]
        + later_sum.reshape(spread) * later_scale[..., None]
    )
    return (
        row_max,
        earlier_total * earlier_scale + later_total * later_scale,
        joined.reshape(earlier_sum.shape),
    )


def block_part(scores, live_mask, block_values):
    seq_count, heads_local, prop_count, key_count = scores.shape
    row_max = jnp.max(scores, axis=3)
    weights = jnp.where(live_mask, jnp.exp(scores - row_max[..., None]), 0.0)
    row_total = jnp.sum(weights, axis=3)
    weighted = jnp.einsum(
        "shpk,skhd->sphd",
        weights.astype(jnp.bfloat16),
        block_values,
        preferred_element_type=jnp.float32,
    )
    return (
        jnp.transpose(row_max, (0, 2, 1)),
        jnp.transpose(row_total, (0, 2, 1)),
        weighted.reshape(seq_count, prop_count, -1),
    )


def finish_rows(row_sums, inverse, query_gain, key_gain, heads_local):
    head_width = row_sums.shape[1] // 3
    head_size = head_width // heads_local
    row_count = row_sums.shape[0]
    raw_sums = row_sums * inverse[:, None]
    queries = head_norm(
        raw_sums[:, :head_width].reshape(row_count, heads_local, head_size), query_gain
    )
    keyed = head_norm(
        raw_sums[:, head_width : 2 * head_width].reshape(row_count, heads_local, head_size),
        key_gain,
    )
    return jnp.concatenate(
        [
            queries.reshape(row_count, head_width),
            keyed.reshape(row_count, head_width),
            raw_sums[:, 2 * head_width :],
        ],
        axis=1,
    ).astype(jnp.bfloat16)


def flatten_part(part_triple, rows_all):
    part_max, part_total, part_sum = part_triple
    return (
        part_max.reshape(rows_all, -1),
        part_total.reshape(rows_all, -1),
        part_sum.reshape(rows_all, -1),
    )


def shards(
    tokens,
    norm_gain,
    w_query,
    w_key,
    w_value,
    w_forget,
    forget_bias,
    query_gain,
    key_gain,
    head_gain,
    w_out,
    key_cache,
    value_cache,
    gate_cache,
    lengths,
    accepted,
    parents,
):
    seq_count, prop_count, width_in = tokens.shape
    pos_dev = key_cache.shape[1]
    heads_local = gate_cache.shape[1]
    head_width = key_cache.shape[2]
    head_size = head_width // heads_local
    rows_all = seq_count * prop_count
    full_width = w_forget.shape[0]
    kv_index = lax.axis_index("kv")
    tp_index = lax.axis_index("tp")
    flattened = tokens.reshape(rows_all, width_in).astype(jnp.float32)
    squares = jnp.sum(flattened * flattened, axis=1)
    scaled = (flattened * norm_gain).astype(jnp.bfloat16)
    w_rows = lax.dynamic_slice_in_dim(w_forget, kv_index * width_in, width_in, 0)
    gate_part = jnp.dot(scaled, w_rows, preferred_element_type=jnp.float32)
    w_joined = jnp.concatenate([w_query, w_key, w_value], axis=1)
    summed, gate_sum, square_sum = lax.psum(
        (jnp.dot(scaled, w_joined, preferred_element_type=jnp.float32), gate_part, squares), "kv"
    )
    inverse = lax.rsqrt(square_sum / full_width + EPSILON)
    joined = finish_rows(summed, inverse, query_gain, key_gain, heads_local)
    log_all = jax.nn.log_sigmoid(gate_sum * inverse[:, None] + forget_bias)
    log_own = lax.dynamic_slice_in_dim(log_all, tp_index * heads_local, heads_local, 1)
    log_own = log_own.reshape(seq_count, prop_count, heads_local)
    queries = joined[:, :head_width].reshape(seq_count, prop_count, heads_local, head_size)
    keys_new = joined[:, head_width : 2 * head_width].reshape(
        seq_count, prop_count, heads_local, head_size
    )
    values_new = joined[:, 2 * head_width :].reshape(seq_count, prop_count, heads_local, head_size)
    ancestors = ancestry(parents)
    path_sum = jnp.einsum("sij,sjh->sih", ancestors, log_own, precision=lax.Precision.HIGHEST)
    base_pos = lengths + accepted
    positions = kv_index * pos_dev + jnp.arange(pos_dev, dtype=jnp.int32)
    score_scale = head_size ** (-0.5)
    cached_keys = key_cache.reshape(seq_count, pos_dev, heads_local, head_size)
    cached_values = value_cache.reshape(seq_count, pos_dev, heads_local, head_size)
    scores = jnp.einsum("sphd,skhd->shpk", queries, cached_keys, preferred_element_type=jnp.float32)
    scores = scores * score_scale - gate_cache[:, :, None, :]
    live_mask = (positions[None, :] < base_pos[:, None])[:, None, None, :]
    scores = jnp.where(live_mask, scores, MASKED)
    local_part = block_part(scores, live_mask, cached_values)
    hit_mask = positions[None, :] == (base_pos - 1)[:, None]
    boundary_local = jnp.sum(jnp.where(hit_mask[:, None, :], gate_cache, 0.0), axis=2)
    tree_live = (ancestors > 0.5)[:, None, :, :]
    boundary = lax.psum(boundary_local, "kv")
    flat_max, flat_total, flat_sum = flatten_part(local_part, rows_all)
    got_max, got_total, got_sum = (
        lax.all_to_all(flat_max[None], "kv", split_axis=1, concat_axis=0, tiled=True),
        lax.all_to_all(flat_total[None], "kv", split_axis=1, concat_axis=0, tiled=True),
        lax.all_to_all(flat_sum[None], "kv", split_axis=1, concat_axis=0, tiled=True),
    )
    top = jnp.max(got_max, axis=0)
    factors = jnp.exp(got_max - top[None])
    own_rows = got_max.shape[1]
    summed_rows = jnp.sum(
        got_sum.reshape(got_sum.shape[0], own_rows, heads_local, head_size) * factors[..., None],
        axis=0,
    )
    merged = (top, jnp.sum(got_total * factors, axis=0), summed_rows.reshape(own_rows, head_width))
    tree_scores = jnp.einsum(
        "sphd,sjhd->shpj", queries, keys_new, preferred_element_type=jnp.float32
    )
    tree_scores = (
        tree_scores * score_scale
        - jnp.transpose(path_sum, (0, 2, 1))[:, :, None, :]
        - boundary[:, :, None, None]
    )
    tree_scores = jnp.where(tree_live, tree_scores, MASKED)
    tree_max, tree_total, tree_sum = flatten_part(
        block_part(tree_scores, tree_live, values_new), rows_all
    )
    row_lower = kv_index * own_rows
    merged = combine(
        merged,
        (
            lax.dynamic_slice_in_dim(tree_max, row_lower, own_rows, 0),
            lax.dynamic_slice_in_dim(tree_total, row_lower, own_rows, 0),
            lax.dynamic_slice_in_dim(tree_sum, row_lower, own_rows, 0),
        ),
    )
    row_max, row_total, weighted = merged
    attended = weighted.reshape(own_rows, heads_local, head_size) / row_total[..., None]
    own_normed = head_norm(attended, head_gain).astype(jnp.bfloat16).reshape(own_rows, head_width)
    normed = lax.all_gather(own_normed, "kv", axis=0, tiled=True)
    out_term = jnp.dot(normed, w_out, preferred_element_type=jnp.float32)
    layer_out = lax.psum(out_term.astype(jnp.bfloat16), "tp")
    layer_out = layer_out.reshape(seq_count, prop_count, -1)
    new_rows = jnp.concatenate(
        [
            keys_new.reshape(seq_count, prop_count, head_width),
            values_new.reshape(seq_count, prop_count, head_width),
        ],
        axis=2,
    )
    slot_index = positions[None, :, None] - base_pos[:, None, None]
    placing = slot_index == jnp.arange(prop_count, dtype=jnp.int32)[None, None, :]
    written = jnp.einsum(
        "skp,spc->skc", placing.astype(jnp.bfloat16), new_rows, preferred_element_type=jnp.float32
    ).astype(jnp.bfloat16)
    hit_rows = jnp.any(placing, axis=2)[..., None]
    new_keys = jnp.where(hit_rows, written[..., :head_width], key_cache)
    new_values = jnp.where(hit_rows, written[..., head_width:], value_cache)
    return (layer_out, new_keys, new_values, log_own)


def solution(mesh):
    placed = (
        P("dp", None, "kv"),
        P("kv"),
        P("kv", "tp"),
        P("kv", "tp"),
        P("kv", "tp"),
        P(),
        P(),
        P(),
        P(),
        P(),
        P("tp", "kv"),
        P("dp", "kv", "tp"),
        P("dp", "kv", "tp"),
        P("dp", "tp", "kv"),
        P("dp"),
        P("dp"),
        P("dp", None),
    )
    return jax.shard_map(
        shards,
        mesh=mesh,
        in_specs=placed,
        out_specs=(
            P("dp", None, "kv"),
            P("dp", "kv", "tp"),
            P("dp", "kv", "tp"),
            P("dp", None, "tp"),
        ),
        check_vma=False,
    )
```

profile of v0, /device:TPU:0, one launch (start us, length us, event | category | flops | bytes accessed | tf_op | source)
XLA Modules:
  0.0 129.3 jit_solution(6320880123169172122)
XLA Ops:
  7.2 0.9 fusion.29
  8.3 2.6 %fusion.6 = f32[64,1536]{1,0:T(8,128)} fusion(bf16[64,512]{1,0:T(8,128)(2,1)S(1)} %fusion.29, bf16[512,512]{1,0:T(8,128)(2,1)} %param.23, bf16[512,512]{1,0:T(8,128)(2,1)} %param.22, bf16[512,512]{1,0:T(8,128)(2,1)} %param.21), kind=kOutput, calls=%fused_computation.9 | convolution fusion | flops 105381888 | bytes 2031616 | tf_op jit(solution)/shard_map/dot_general | solution.py:131
  11.2 4.2 %while.11 = (s32[]{:T(128)}, f32[4,16,16]{2,1,0:T(8,128)S(1)}, s32[4,16]{1,0:T(4,128)S(1)}, f32[16,16]{1,0:T(8,128)S(1)}, s32[]{:T(128)}) while((s32[]{:T(128)}, f32[4,16,16]{2,1,0:T(8,128)S(1)}, s32[4,16]{1,0:T(4,128)S(1)}, f32[16,16]{1,0:T(8,128)S(1)}, s32[]{:T(128)}) %tuple.50), condition=%wide.region_8.9_spmd.clone, body=%wide.region_7.8_spmd.clone.sunk | while | flops 199682 | bytes 17725 | solution.py:26
  11.3 0.2 convolution_add_fusion.2
  11.5 0.2 convolution_add_fusion.2
  11.8 0.2 convolution_add_fusion.2
  12.1 0.2 convolution_add_fusion.2
  12.3 0.2 convolution_add_fusion.2
  12.6 0.2 convolution_add_fusion.2
  12.8 0.2 convolution_add_fusion.2
  13.1 0.2 convolution_add_fusion.2
  13.4 0.2 convolution_add_fusion.2
  13.6 0.2 convolution_add_fusion.2
  13.9 0.2 convolution_add_fusion.2
  14.2 0.2 convolution_add_fusion.2
  14.4 0.2 convolution_add_fusion.2
  14.7 0.2 convolution_add_fusion.2
  15.0 0.2 convolution_add_fusion.2
  15.2 0.2 convolution_add_fusion.2
  15.6 0.8 fusion.39
  16.4 20.4 %all-reduce = (f32[64]{0:T(128)S(1)}, f32[4,8]{1,0:T(4,128)S(1)}, f32[64,16]{0,1:T(8,128)S(1)}) all-reduce(f32[64]{0:T(128)S(1)} %reduce_sum.86, f32[4,8]{1,0:T(4,128)S(1)} %select_reduce_fusion, f32[64,16]{0,1:T(8,128)S(1)} %fusion.39), channel_id=1, replica_groups=mesh['dp'=4,'kv'=4,'tp'=2] {'kv'}, use_global_device_ids=true, to_apply=%region_2.0 | all-reduce | flops 1120 | bytes 8960 | tf_op jit(solution)/shard_map/psum | solution.py:130
  37.4 4.3 %copy.136 = bf16[4,512,512]{1,2,0:T(8,128)(2,1)} copy(bf16[4,512,512]{2,1,0:T(8,128)(2,1)} %param.30) | data formatting | bytes 4194304 | tf_op args[11]
  41.7 2.4 %copy.138 = bf16[4,512,512]{1,2,0:T(8,128)(2,1)} copy(bf16[4,512,512]{2,1,0:T(8,128)(2,1)S(1)} %copy-done.1) | data formatting | bytes 4194304 | tf_op args[12]
  44.1 0.2 fusion.58
  44.3 6.7 %all-reduce.4.cloned.1.call-done = f32[64,1536]{1,0:T(8,128)} async-done(((f32[64,1536]{1,0:T(8,128)}), f32[64,1536]{1,0:T(8,128)}) %all-reduce.4.cloned.1.call-update) | async-done | bytes 393232 | tf_op jit(solution)/shard_map/psum | solution.py:130
  51.0 1.1 broadcast_multiply_fusion
  52.1 0.1 reshape.236
  52.4 0.1 reduce_sum.87
  52.7 0.1 mul.203
  52.8 0.1 mul.204
  53.1 0.1 reduce_sum.89
  53.4 0.1 mul.217
  53.5 0.1 mul.218
  53.7 0.1 reshape.230
  53.8 0.1 reshape.233
  53.9 2.1 %fusion.57 = (f32[4,8,16]{2,1,0:T(8,128)S(1)}, f32[4,8,16,512]{3,2,1,0:T(8,128)S(1)}) fusion(f32[4,8,512]{2,1,0:T(8,128)S(1)} %copy-done.3, bf16[4,512,8,64]{1,3,2,0:T(8,128)(2,1)} %bitcast.48, bf16[4,16,8,64]{3,2,1,0:T(8,128)(2,1)S(1)} %reshape.230, pred[4,512]{1,0:T(4,128)(4,1)S(1)} %get-tuple-element.90), kind=kOutput, calls=%fused_computation.96 | convolution fusion | flops 34602496 | bytes 3280896 | tf_op jit(solution)/shard_map/sphd,skhd->shpk/dot_general | solution.py:150
  56.0 0.3 fusion.17
  56.4 0.5 broadcast.155
  57.0 0.7 reduce.2
  57.7 0.7 reshape.243
  58.3 3.4 %all-to-all-start.2 = ((f32[4,1,128]{2,1,0:T(1,128)}), f32[4,1,128]{2,1,0:T(1,128)S(1)}, u32[]{:S(2)}, u32[]{:S(2)}) async-start(f32[4,1,128]{2,1,0:T(1,128)} %reshape.243), calls=%async_computation.2 | async-start | bytes 4096 | tf_op jit(solution)/shard_map/all_to_all | solution.py:162
  61.8 2.3 %convolution_bitcast_fusion = f32[4,16,8,64]{3,1,2,0:T(8,128)S(1)} fusion(bf16[4,512,8,64]{1,3,2,0:T(8,128)(2,1)} %bitcast.47, f32[4,8,16,512]{3,2,1,0:T(8,128)S(1)} %get-tuple-element.95, f32[4,8,16]{2,1,0:T(8,128)S(1)} %get-tuple-element.94, pred[4,512]{1,0:T(4,128)(4,1)S(1)} %get-tuple-element.90), kind=kOutput, calls=%fused_computation.21 | convolution fusion | flops 34340864 | bytes 3280896 | tf_op jit(solution)/shard_map/shpk,skhd->sphd/dot_general | solution.py:52
  64.1 3.2 %convolution_convert_fusion = bf16[4,512,1024]{2,1,0:T(8,128)(2,1)} fusion(bf16[4,16,512]{2,1,0:T(8,128)(2,1)S(1)} %bitcast.50, bf16[4,16,512]{2,1,0:T(8,128)(2,1)S(1)} %bitcast.49, s32[4,512]{1,0:T(4,128)S(1)} %broadcast_subtract_fusion), kind=kOutput, calls=%fused_computation.6 | convolution fusion | flops 69500928 | bytes 4333568 | tf_op jit(solution)/shard_map/skp,spc->skc/dot_general | solution.py:210
  67.3 0.2 fusion.56
  67.6 0.2 convolution_bitcast_fusion.1
  68.0 0.1 reshape_reshape.9
  68.2 0.7 reduce.4
  68.9 0.7 reshape.241
  69.6 5.1 %all-to-all-start.1 = ((f32[4,1,128]{2,1,0:T(1,128)}), f32[4,1,128]{2,1,0:T(1,128)S(1)}, u32[]{:S(2)}, u32[]{:S(2)}) async-start(f32[4,1,128]{2,1,0:T(1,128)} %reshape.241), calls=%async_computation.1 | async-start | bytes 4096 | tf_op jit(solution)/shard_map/all_to_all | solution.py:161
  75.0 0.8 broadcast_in_dim_reshape_reshape.4
  75.8 0.6 reduce.3
  76.6 3.6 %all-to-all-done.1 = f32[4,1,128]{2,1,0:T(1,128)S(1)} async-done(((f32[4,1,128]{2,1,0:T(1,128)}), f32[4,1,128]{2,1,0:T(1,128)S(1)}, u32[]{:S(2)}, u32[]{:S(2)}) %all-to-all-start.1) | async-done | bytes 2080 | tf_op jit(solution)/shard_map/all_to_all | solution.py:161
  80.1 3.3 %all-to-all-start = ((f32[1,64,512]{2,0,1:T(1,128)}), f32[1,64,512]{2,0,1:T(1,128)S(1)}, u32[]{:S(2)}, u32[]{:S(2)}) async-start(f32[1,64,512]{2,0,1:T(1,128)} %broadcast_in_dim_reshape_reshape.4), calls=%async_computation | async-start | bytes 262144 | tf_op jit(solution)/shard_map/all_to_all | solution.py:163
  83.5 0.6 reduce.5
  84.8 0.1 mul.212
  85.0 0.2 mul.213
  85.2 4.2 %all-to-all-done = f32[1,64,512]{2,0,1:T(1,128)S(1)} async-done(((f32[1,64,512]{2,0,1:T(1,128)}), f32[1,64,512]{2,0,1:T(1,128)S(1)}, u32[]{:S(2)}, u32[]{:S(2)}) %all-to-all-start) | async-done | bytes 131104 | tf_op jit(solution)/shard_map/all_to_all | solution.py:163
  89.4 0.2 multiply_reduce_fusion
  89.7 0.2 multiply_reduce_fusion.2
  90.1 13.1 %all_gather.3 = bf16[64,512]{1,0:T(8,128)(2,1)S(1)} all-gather(bf16[16,512]{1,0:T(8,128)(2,1)S(1)} %multiply_convert_fusion.2), channel_id=1, replica_groups=mesh['dp'=4,'kv'=4,'tp'=2] {'kv'}, dimensions={0}, use_global_device_ids=true | all-gather | bytes 81920 | tf_op jit(solution)/shard_map/all_gather | solution.py:197
  103.2 0.8 convolution_convert_fusion.1
  104.1 4.4 %slice_select_fusion = (bf16[4,512,512]{2,1,0:T(8,128)(2,1)}, bf16[4,512,512]{2,1,0:T(8,128)(2,1)}) fusion(bf16[4,512,512]{2,1,0:T(8,128)(2,1)S(1)} %copy-done.2, bf16[4,512,1024]{2,1,0:T(8,128)(2,1)} %convolution_convert_fusion, pred[4,512]{1,0:T(4,128)(4,1)S(1)} %fusion.32, bf16[4,512,512]{2,1,0:T(8,128)(2,1)} %param.30), kind=kLoop, calls=%fused_computation.7 | loop fusion | flops 2097152 | bytes 12584960 | tf_op jit(solution)/shard_map/jit(_where)/select_n | solution.py:215
  108.5 12.4 %all-reduce.6.cloned.1.call-done = bf16[4,16,512]{2,1,0:T(8,128)(2,1)} async-done(((bf16[4,16,512]{2,1,0:T(8,128)(2,1)}), bf16[4,16,512]{2,1,0:T(8,128)(2,1)}) %all-reduce.6.cloned.1.call-update) | async-done | bytes 65552 | tf_op jit(solution)/shard_map/psum | solution.py:199
  121.0 1.5 %copy.192 = bf16[4,16,512]{2,1,0:T(8,128)(2,1)} copy(bf16[4,16,512]{2,1,0:T(8,128)(2,1)} %all-reduce.6.cloned.1.call-done) | data formatting | bytes 131072
  (106 shorter events, 3.5 us)
Async XLA Ops:
  7.2 96.0 %copy-start = (bf16[512,512]{1,0:T(8,128)(2,1)S(1)}, bf16[512,512]{1,0:T(8,128)(2,1)}, u32[]{:S(2)}) copy-start(bf16[512,512]{1,0:T(8,128)(2,1)} %param.29) | copy-start | bytes 1572868
  7.2 43.8 %all-reduce.4.cloned.1.call-start = ((), (), s32[]{:S(2)}) async-start(), calls=%async_computation.3 | async-start | bytes 786432 | tf_op jit(solution)/shard_map/psum | solution.py:130
  8.1 2.7 %copy-start.4 = (bf16[4,16,512]{2,1,0:T(8,128)(2,1)S(1)}, bf16[4,16,512]{2,1,0:T(8,128)(2,1)}, u32[]{:S(2)}) copy-start(bf16[4,16,512]{2,1,0:T(8,128)(2,1)} %param.19) | copy-start | bytes 196612
  8.2 2.9 %copy-start.11 = (s32[4]{0:T(128)S(1)}, s32[4]{0:T(128)}, u32[]{:S(2)}) copy-start(s32[4]{0:T(128)} %param.33) | copy-start | bytes 52
  8.2 2.9 %copy-start.12 = (s32[4]{0:T(128)S(1)}, s32[4]{0:T(128)}, u32[]{:S(2)}) copy-start(s32[4]{0:T(128)} %param.34) | copy-start | bytes 52
  8.2 3.0 %copy-start.6 = (s32[4,16]{1,0:T(4,128)S(1)}, s32[4,16]{1,0:T(4,128)}, u32[]{:S(2)}) copy-start(s32[4,16]{1,0:T(4,128)} %param.35) | copy-start | bytes 772
  8.2 7.3 %copy-start.3 = (f32[4,8,512]{2,1,0:T(8,128)S(1)}, f32[4,8,512]{2,1,0:T(8,128)}, u32[]{:S(2)}) copy-start(f32[4,8,512]{2,1,0:T(8,128)} %param.32) | copy-start | bytes 196612
  8.2 28.7 %copy-start.7 = (f32[16]{0:T(128)S(1)}, f32[16]{0:T(128)}, u32[]{:S(2)}) copy-start(f32[16]{0:T(128)} %param.25) | copy-start | bytes 196
  8.2 28.8 %copy-start.8 = (f32[64]{0:T(128)S(1)}, f32[64]{0:T(128)}, u32[]{:S(2)}) copy-start(f32[64]{0:T(128)} %param.26) | copy-start | bytes 772
  8.2 28.8 %copy-start.9 = (f32[64]{0:T(128)S(1)}, f32[64]{0:T(128)}, u32[]{:S(2)}) copy-start(f32[64]{0:T(128)} %param.27) | copy-start | bytes 772
  8.2 28.9 %copy-start.10 = (f32[64]{0:T(128)S(1)}, f32[64]{0:T(128)}, u32[]{:S(2)}) copy-start(f32[64]{0:T(128)} %param.28) | copy-start | bytes 772
  37.4 6.7 %copy-start.5 = (f32[4,16,8]{1,2,0:T(8,128)}, f32[4,16,8]{1,2,0:T(8,128)S(1)}, u32[]{:S(2)}) copy-start(f32[4,16,8]{1,2,0:T(8,128)S(1)} %copy.148) | copy-start | bytes 6148
  37.4 4.3 %copy-start.1 = (bf16[4,512,512]{2,1,0:T(8,128)(2,1)S(1)}, bf16[4,512,512]{2,1,0:T(8,128)(2,1)}, u32[]{:S(2)}) copy-start(bf16[4,512,512]{2,1,0:T(8,128)(2,1)} %param.31) | copy-start | bytes 6291460
  58.3 11.2 %all-to-all-start.2 = ((f32[4,1,128]{2,1,0:T(1,128)}), f32[4,1,128]{2,1,0:T(1,128)S(1)}, u32[]{:S(2)}, u32[]{:S(2)}) async-start(f32[4,1,128]{2,1,0:T(1,128)} %reshape.243), calls=%async_computation.2 | async-start | bytes 4096 | tf_op jit(solution)/shard_map/all_to_all | solution.py:162
  69.6 10.6 %all-to-all-start.1 = ((f32[4,1,128]{2,1,0:T(1,128)}), f32[4,1,128]{2,1,0:T(1,128)S(1)}, u32[]{:S(2)}, u32[]{:S(2)}) async-start(f32[4,1,128]{2,1,0:T(1,128)} %reshape.241), calls=%async_computation.1 | async-start | bytes 4096 | tf_op jit(solution)/shard_map/all_to_all | solution.py:161
  75.0 29.1 %copy-start.2 = (bf16[4,512,512]{2,1,0:T(8,128)(2,1)S(1)}, bf16[4,512,512]{2,1,0:T(8,128)(2,1)}, u32[]{:S(2)}) copy-start(bf16[4,512,512]{2,1,0:T(8,128)(2,1)} %param.31) | copy-start | bytes 6291460
  80.1 9.2 %all-to-all-start = ((f32[1,64,512]{2,0,1:T(1,128)}), f32[1,64,512]{2,0,1:T(1,128)S(1)}, u32[]{:S(2)}, u32[]{:S(2)}) async-start(f32[1,64,512]{2,0,1:T(1,128)} %broadcast_in_dim_reshape_reshape.4), calls=%async_computation | async-start | bytes 262144 | tf_op jit(solution)/shard_map/all_to_all | solution.py:163
  83.5 37.5 %all-reduce.6.cloned.1.call-start = ((), (), s32[]{:S(2)}) async-start(), calls=%async_computation.4 | async-start | bytes 131072 | tf_op jit(solution)/shard_map/psum | solution.py:199
Sparse Core Ops, SparseCore 0:
  11.0 39.9 all-reduce.3
  104.2 16.7 all-reduce.5
where the time goes:
time: 130 us; the launch traced here: 129 us
  blocking collectives  33.6 us (26%)
  waiting for transfers between devices  27 us (21%)
  matrix products  16.2 us (12%)
  local copies, waits for them, and re-layouts  14.8 us (11%)
  between operations  14.5 us (11%)
  starting transfers between devices  11.9 us (9%)
  other arithmetic  10.9 us (8%)
    psum x1, blocking collectives, shards(): lax.psum((jnp.dot(scaled, w_joined, preferred_element_type=jnp.float32),...  20.4 us
    all_gather x1, blocking collectives, shards(): normed = lax.all_gather(own_normed, 'kv', axis=0, tiled=True)  13.1 us
    psum x1, waiting for transfers between devices, shards(): layer_out = lax.psum(out_term.astype(jnp.bfloat16), 'tp')  12.4 us
    unnamed x34, local copies, waits for them, and re-layouts  10.3 us
    psum x1, waiting for transfers between devices, shards(): lax.psum((jnp.dot(scaled, w_joined, preferred_element_type=jnp.float32),...  6.72 us
    all_to_all x1, starting transfers between devices, shards(): lax.all_to_all(flat_max[None], 'kv', split_axis=1, concat_axis=0, tiled=T...  5.09 us
    select_n x1, other arithmetic, shards(): new_values = jnp.where(hit_rows, written[..., head_width:], value_cache)  4.45 us
    all_to_all x1, waiting for transfers between devices, shards(): lax.all_to_all(flat_sum[None], 'kv', split_axis=1, concat_axis=0, tiled=T...  4.2 us
  transfers between devices with their start and end apart: 5, of which 4 were waited for; matrix products, arithmetic and copies ran while one was open for 22% of the time, Pallas kernels for 0%

commit v1 on v0

--- a/solution.py
+++ b/solution.py
@@ -158,7 +158,12 @@
     boundary = lax.psum(boundary_local, "kv")
     flat_max, flat_total, flat_sum = flatten_part(local_part, rows_all)
     got_max, got_total, got_sum = (
-        lax.all_to_all(flat_max[None], "kv", split_axis=1, concat_axis=0, tiled=True),
+        jnp.concatenate(
+            lax.all_to_all(
+                jnp.stack(jnp.split(flat_max[None], lax.axis_size("kv"), axis=1)), "kv", 0, 0
+            ),
+            axis=0,
+        ),
         lax.all_to_all(flat_total[None], "kv", split_axis=1, concat_axis=0, tiled=True),
         lax.all_to_all(flat_sum[None], "kv", split_axis=1, concat_axis=0, tiled=True),
     )

time: 130 us -> 131 us (level)
    all_to_all x1, waiting for transfers between devices: 0.01 us -> 4.77 us  [shards(): lax.all_to_all(flat_total[None], 'kv', split_axis=1, concat_axis=0, tiled...]
    all_to_all x1, waiting for transfers between devices: 3.58 us -> 0.01 us  [shards(): lax.all_to_all(jnp.stack(jnp.split(flat_max[None], lax.axis_size('kv'), a...]
    all_to_all x1, starting transfers between devices: 3.44 us -> 5.09 us  [shards(): lax.all_to_all(flat_total[None], 'kv', split_axis=1, concat_axis=0, tiled...]
    all_to_all x1, starting transfers between devices: 5.09 us -> 3.43 us  [shards(): lax.all_to_all(jnp.stack(jnp.split(flat_max[None], lax.axis_size('kv'), a...]
where the time goes in v1:
time: 131 us; the launch traced here: 130 us
  blocking collectives  33.6 us (26%)
  waiting for transfers between devices  27.8 us (21%)
  matrix products  16.2 us (12%)
  local copies, waits for them, and re-layouts  15.2 us (12%)
  between operations  14.5 us (11%)
  starting transfers between devices  11.9 us (9%)
  other arithmetic  10.2 us (8%)
    psum x1, blocking collectives, shards(): lax.psum((jnp.dot(scaled, w_joined, preferred_element_type=jnp.float32),...  20.4 us
    all_gather x1, blocking collectives, shards(): normed = lax.all_gather(own_normed, 'kv', axis=0, tiled=True)  13.1 us
    psum x1, waiting for transfers between devices, shards(): layer_out = lax.psum(out_term.astype(jnp.bfloat16), 'tp')  12.4 us
    unnamed x34, local copies, waits for them, and re-layouts  10.3 us
    psum x1, waiting for transfers between devices, shards(): lax.psum((jnp.dot(scaled, w_joined, preferred_element_type=jnp.float32),...  6.72 us
    all_to_all x1, starting transfers between devices, shards(): lax.all_to_all(flat_total[None], 'kv', split_axis=1, concat_axis=0, tiled...  5.09 us
    all_to_all x1, waiting for transfers between devices, shards(): lax.all_to_all(flat_total[None], 'kv', split_axis=1, concat_axis=0, tiled...  4.77 us
    select_n x1, other arithmetic, shards(): new_values = jnp.where(hit_rows, written[..., head_width:], value_cache)  4.45 us
  transfers between devices with their start and end apart: 5, of which 4 were waited for; matrix products, arithmetic and copies ran while one was open for 22% of the time, Pallas kernels for 0%

profile of v1, /device:TPU:0, one launch (start us, length us, event | category | flops | bytes accessed | tf_op | source)
XLA Modules:
  0.0 129.8 jit_solution(11201349422121988197)
XLA Ops:
  7.2 0.9 fusion.29
  8.3 2.6 %fusion.6 = f32[64,1536]{1,0:T(8,128)} fusion(bf16[64,512]{1,0:T(8,128)(2,1)S(1)} %fusion.29, bf16[512,512]{1,0:T(8,128)(2,1)} %param.23, bf16[512,512]{1,0:T(8,128)(2,1)} %param.22, bf16[512,512]{1,0:T(8,128)(2,1)} %param.21), kind=kOutput, calls=%fused_computation.9 | convolution fusion | flops 105381888 | bytes 2031616 | tf_op jit(solution)/shard_map/dot_general | solution.py:131
  11.2 4.2 %while.11 = (s32[]{:T(128)}, f32[4,16,16]{2,1,0:T(8,128)S(1)}, s32[4,16]{1,0:T(4,128)S(1)}, f32[16,16]{1,0:T(8,128)S(1)}, s32[]{:T(128)}) while((s32[]{:T(128)}, f32[4,16,16]{2,1,0:T(8,128)S(1)}, s32[4,16]{1,0:T(4,128)S(1)}, f32[16,16]{1,0:T(8,128)S(1)}, s32[]{:T(128)}) %tuple.52), condition=%wide.region_8.9_spmd.clone, body=%wide.region_7.8_spmd.clone.sunk | while | flops 199682 | bytes 17725 | solution.py:26
  11.3 0.2 convolution_add_fusion.2
  11.5 0.2 convolution_add_fusion.2
  11.8 0.2 convolution_add_fusion.2
  12.1 0.2 convolution_add_fusion.2
  12.3 0.2 convolution_add_fusion.2
  12.6 0.2 convolution_add_fusion.2
  12.8 0.2 convolution_add_fusion.2
  13.1 0.2 convolution_add_fusion.2
  13.4 0.2 convolution_add_fusion.2
  13.6 0.2 convolution_add_fusion.2
  13.9 0.2 convolution_add_fusion.2
  14.2 0.2 convolution_add_fusion.2
  14.4 0.2 convolution_add_fusion.2
  14.7 0.2 convolution_add_fusion.2
  15.0 0.2 convolution_add_fusion.2
  15.2 0.2 convolution_add_fusion.2
  15.6 0.8 fusion.40
  16.4 20.4 %all-reduce = (f32[64]{0:T(128)S(1)}, f32[4,8]{1,0:T(4,128)S(1)}, f32[64,16]{0,1:T(8,128)S(1)}) all-reduce(f32[64]{0:T(128)S(1)} %reduce_sum.86, f32[4,8]{1,0:T(4,128)S(1)} %select_reduce_fusion, f32[64,16]{0,1:T(8,128)S(1)} %fusion.40), channel_id=1, replica_groups=mesh['dp'=4,'kv'=4,'tp'=2] {'kv'}, use_global_device_ids=true, to_apply=%region_2.0 | all-reduce | flops 1120 | bytes 8960 | tf_op jit(solution)/shard_map/psum | solution.py:130
  37.4 4.3 %copy.128 = bf16[4,512,512]{1,2,0:T(8,128)(2,1)} copy(bf16[4,512,512]{2,1,0:T(8,128)(2,1)} %param.30) | data formatting | bytes 4194304 | tf_op args[11]
  41.7 2.4 %copy.130 = bf16[4,512,512]{1,2,0:T(8,128)(2,1)} copy(bf16[4,512,512]{2,1,0:T(8,128)(2,1)S(1)} %copy-done.1) | data formatting | bytes 4194304 | tf_op args[12]
  44.1 0.2 fusion.61
  44.3 6.7 %all-reduce.4.cloned.1.call-done = f32[64,1536]{1,0:T(8,128)} async-done(((f32[64,1536]{1,0:T(8,128)}), f32[64,1536]{1,0:T(8,128)}) %all-reduce.4.cloned.1.call-update) | async-done | bytes 393232 | tf_op jit(solution)/shard_map/psum | solution.py:130
  51.0 1.1 broadcast_multiply_fusion
  52.1 0.1 reshape.240
  52.4 0.1 reduce_sum.87
  52.7 0.1 mul.203
  52.8 0.1 mul.204
  53.1 0.1 reduce_sum.89
  53.4 0.1 mul.217
  53.5 0.1 mul.218
  53.7 0.1 reshape.233
  53.8 0.1 reshape.237
  53.9 0.2 fusion.58
  54.3 0.2 convolution_bitcast_fusion.1
  54.6 0.1 reshape_reshape.9
  54.7 2.1 %fusion.59 = (f32[4,8,16]{2,1,0:T(8,128)S(1)}, f32[4,8,16,512]{3,2,1,0:T(8,128)S(1)}) fusion(f32[4,8,512]{2,1,0:T(8,128)S(1)} %copy-done.3, bf16[4,512,8,64]{1,3,2,0:T(8,128)(2,1)} %bitcast.66, bf16[4,16,8,64]{3,2,1,0:T(8,128)(2,1)S(1)} %reshape.233, pred[4,512]{1,0:T(4,128)(4,1)S(1)} %get-tuple-element.90), kind=kOutput, calls=%fused_computation.102 | convolution fusion | flops 34602496 | bytes 3280896 | tf_op jit(solution)/shard_map/sphd,skhd->shpk/dot_general | solution.py:150
  57.0 0.7 reshape.245
  57.7 3.4 %all-to-all-start.1 = ((f32[4,1,128]{2,1,0:T(1,128)}), f32[4,1,128]{2,1,0:T(1,128)S(1)}, u32[]{:S(2)}, u32[]{:S(2)}) async-start(f32[4,1,128]{2,1,0:T(1,128)} %reshape.245), calls=%async_computation.1 | async-start | bytes 4096 | tf_op jit(solution)/shard_map/all_to_all | solution.py:162
  61.1 0.3 fusion.17
  61.4 2.3 %convolution_bitcast_fusion = f32[4,16,8,64]{3,1,2,0:T(8,128)S(1)} fusion(bf16[4,512,8,64]{1,3,2,0:T(8,128)(2,1)} %bitcast.65, f32[4,8,16,512]{3,2,1,0:T(8,128)S(1)} %get-tuple-element.95, f32[4,8,16]{2,1,0:T(8,128)S(1)} %get-tuple-element.94, pred[4,512]{1,0:T(4,128)(4,1)S(1)} %get-tuple-element.90), kind=kOutput, calls=%fused_computation.21 | convolution fusion | flops 34340864 | bytes 3280896 | tf_op jit(solution)/shard_map/shpk,skhd->sphd/dot_general | solution.py:52
  63.7 3.2 %convolution_convert_fusion = bf16[4,512,1024]{2,1,0:T(8,128)(2,1)} fusion(bf16[4,16,512]{2,1,0:T(8,128)(2,1)S(1)} %bitcast.68, bf16[4,16,512]{2,1,0:T(8,128)(2,1)S(1)} %bitcast.67, s32[4,512]{1,0:T(4,128)S(1)} %broadcast_subtract_fusion), kind=kOutput, calls=%fused_computation.6 | convolution fusion | flops 69500928 | bytes 4333568 | tf_op jit(solution)/shard_map/skp,spc->skc/dot_general | solution.py:215
  67.3 0.5 broadcast.155
  67.8 0.7 reduce.3
  68.5 0.7 reshape.247
  69.3 0.8 broadcast_in_dim_reshape_reshape.4
  70.1 5.1 %all-to-all-start.2 = ((f32[4,1,128]{2,1,0:T(1,128)}), f32[4,1,128]{2,1,0:T(1,128)S(1)}, u32[]{:S(2)}, u32[]{:S(2)}) async-start(f32[4,1,128]{2,1,0:T(1,128)} %reshape.247), calls=%async_computation.2 | async-start | bytes 4096 | tf_op jit(solution)/shard_map/all_to_all | solution.py:167
  75.2 0.6 reduce.5
  76.0 4.8 %all-to-all-done.2 = f32[4,1,128]{2,1,0:T(1,128)S(1)} async-done(((f32[4,1,128]{2,1,0:T(1,128)}), f32[4,1,128]{2,1,0:T(1,128)S(1)}, u32[]{:S(2)}, u32[]{:S(2)}) %all-to-all-start.2) | async-done | bytes 2080 | tf_op jit(solution)/shard_map/all_to_all | solution.py:167
  80.7 3.3 %all-to-all-start = ((f32[1,64,512]{2,0,1:T(1,128)}), f32[1,64,512]{2,0,1:T(1,128)S(1)}, u32[]{:S(2)}, u32[]{:S(2)}) async-start(f32[1,64,512]{2,0,1:T(1,128)} %broadcast_in_dim_reshape_reshape.4), calls=%async_computation | async-start | bytes 262144 | tf_op jit(solution)/shard_map/all_to_all | solution.py:168
  84.1 0.6 reduce.4
  84.7 0.1 reshape.248
  85.8 0.1 mul.212
  86.0 0.2 mul.213
  86.2 3.8 %all-to-all-done = f32[1,64,512]{2,0,1:T(1,128)S(1)} async-done(((f32[1,64,512]{2,0,1:T(1,128)}), f32[1,64,512]{2,0,1:T(1,128)S(1)}, u32[]{:S(2)}, u32[]{:S(2)}) %all-to-all-start) | async-done | bytes 131104 | tf_op jit(solution)/shard_map/all_to_all | solution.py:168
  89.9 0.2 multiply_reduce_fusion
  90.2 0.2 multiply_reduce_fusion.2
  90.6 13.1 %all_gather.3 = bf16[64,512]{1,0:T(8,128)(2,1)S(1)} all-gather(bf16[16,512]{1,0:T(8,128)(2,1)S(1)} %multiply_convert_fusion.2), channel_id=1, replica_groups=mesh['dp'=4,'kv'=4,'tp'=2] {'kv'}, dimensions={0}, use_global_device_ids=true | all-gather | bytes 81920 | tf_op jit(solution)/shard_map/all_gather | solution.py:202
  103.8 0.8 convolution_convert_fusion.1
  104.6 4.4 %slice_select_fusion = (bf16[4,512,512]{2,1,0:T(8,128)(2,1)}, bf16[4,512,512]{2,1,0:T(8,128)(2,1)}) fusion(bf16[4,512,512]{2,1,0:T(8,128)(2,1)S(1)} %copy-done.2, bf16[4,512,1024]{2,1,0:T(8,128)(2,1)} %convolution_convert_fusion, pred[4,512]{1,0:T(4,128)(4,1)S(1)} %fusion.32, bf16[4,512,512]{2,1,0:T(8,128)(2,1)} %param.30), kind=kLoop, calls=%fused_computation.7 | loop fusion | flops 2097152 | bytes 12584960 | tf_op jit(solution)/shard_map/jit(_where)/select_n | solution.py:220
  109.1 12.4 %all-reduce.6.cloned.1.call-done = bf16[4,16,512]{2,1,0:T(8,128)(2,1)} async-done(((bf16[4,16,512]{2,1,0:T(8,128)(2,1)}), bf16[4,16,512]{2,1,0:T(8,128)(2,1)}) %all-reduce.6.cloned.1.call-update) | async-done | bytes 65552 | tf_op jit(solution)/shard_map/psum | solution.py:204
  121.5 1.5 %copy.183 = bf16[4,16,512]{2,1,0:T(8,128)(2,1)} copy(bf16[4,16,512]{2,1,0:T(8,128)(2,1)} %all-reduce.6.cloned.1.call-done) | data formatting | bytes 131072
  (115 shorter events, 3.9 us)
Async XLA Ops:
  7.2 96.6 %copy-start = (bf16[512,512]{1,0:T(8,128)(2,1)S(1)}, bf16[512,512]{1,0:T(8,128)(2,1)}, u32[]{:S(2)}) copy-start(bf16[512,512]{1,0:T(8,128)(2,1)} %param.29) | copy-start | bytes 1572868
  7.2 43.8 %all-reduce.4.cloned.1.call-start = ((), (), s32[]{:S(2)}) async-start(), calls=%async_computation.3 | async-start | bytes 786432 | tf_op jit(solution)/shard_map/psum | solution.py:130
  8.1 2.7 %copy-start.4 = (bf16[4,16,512]{2,1,0:T(8,128)(2,1)S(1)}, bf16[4,16,512]{2,1,0:T(8,128)(2,1)}, u32[]{:S(2)}) copy-start(bf16[4,16,512]{2,1,0:T(8,128)(2,1)} %param.19) | copy-start | bytes 196612
  8.2 2.9 %copy-start.11 = (s32[4]{0:T(128)S(1)}, s32[4]{0:T(128)}, u32[]{:S(2)}) copy-start(s32[4]{0:T(128)} %param.33) | copy-start | bytes 52
  8.2 2.9 %copy-start.12 = (s32[4]{0:T(128)S(1)}, s32[4]{0:T(128)}, u32[]{:S(2)}) copy-start(s32[4]{0:T(128)} %param.34) | copy-start | bytes 52
  8.2 3.0 %copy-start.6 = (s32[4,16]{1,0:T(4,128)S(1)}, s32[4,16]{1,0:T(4,128)}, u32[]{:S(2)}) copy-start(s32[4,16]{1,0:T(4,128)} %param.35) | copy-start | bytes 772
  8.2 7.3 %copy-start.3 = (f32[4,8,512]{2,1,0:T(8,128)S(1)}, f32[4,8,512]{2,1,0:T(8,128)}, u32[]{:S(2)}) copy-start(f32[4,8,512]{2,1,0:T(8,128)} %param.32) | copy-start | bytes 196612
  8.2 28.7 %copy-start.7 = (f32[16]{0:T(128)S(1)}, f32[16]{0:T(128)}, u32[]{:S(2)}) copy-start(f32[16]{0:T(128)} %param.25) | copy-start | bytes 196
  8.2 28.8 %copy-start.8 = (f32[64]{0:T(128)S(1)}, f32[64]{0:T(128)}, u32[]{:S(2)}) copy-start(f32[64]{0:T(128)} %param.26) | copy-start | bytes 772
  8.2 28.8 %copy-start.9 = (f32[64]{0:T(128)S(1)}, f32[64]{0:T(128)}, u32[]{:S(2)}) copy-start(f32[64]{0:T(128)} %param.27) | copy-start | bytes 772
  8.2 28.9 %copy-start.10 = (f32[64]{0:T(128)S(1)}, f32[64]{0:T(128)}, u32[]{:S(2)}) copy-start(f32[64]{0:T(128)} %param.28) | copy-start | bytes 772
  37.4 6.7 %copy-start.5 = (f32[4,16,8]{1,2,0:T(8,128)}, f32[4,16,8]{1,2,0:T(8,128)S(1)}, u32[]{:S(2)}) copy-start(f32[4,16,8]{1,2,0:T(8,128)S(1)} %copy.140) | copy-start | bytes 6148
  37.4 4.3 %copy-start.1 = (bf16[4,512,512]{2,1,0:T(8,128)(2,1)S(1)}, bf16[4,512,512]{2,1,0:T(8,128)(2,1)}, u32[]{:S(2)}) copy-start(bf16[4,512,512]{2,1,0:T(8,128)(2,1)} %param.31) | copy-start | bytes 6291460
  57.7 12.5 %all-to-all-start.1 = ((f32[4,1,128]{2,1,0:T(1,128)}), f32[4,1,128]{2,1,0:T(1,128)S(1)}, u32[]{:S(2)}, u32[]{:S(2)}) async-start(f32[4,1,128]{2,1,0:T(1,128)} %reshape.245), calls=%async_computation.1 | async-start | bytes 4096 | tf_op jit(solution)/shard_map/all_to_all | solution.py:162
  69.3 35.3 %copy-start.2 = (bf16[4,512,512]{2,1,0:T(8,128)(2,1)S(1)}, bf16[4,512,512]{2,1,0:T(8,128)(2,1)}, u32[]{:S(2)}) copy-start(bf16[4,512,512]{2,1,0:T(8,128)(2,1)} %param.31) | copy-start | bytes 6291460
  70.1 10.6 %all-to-all-start.2 = ((f32[4,1,128]{2,1,0:T(1,128)}), f32[4,1,128]{2,1,0:T(1,128)S(1)}, u32[]{:S(2)}, u32[]{:S(2)}) async-start(f32[4,1,128]{2,1,0:T(1,128)} %reshape.247), calls=%async_computation.2 | async-start | bytes 4096 | tf_op jit(solution)/shard_map/all_to_all | solution.py:167
  80.7 9.2 %all-to-all-start = ((f32[1,64,512]{2,0,1:T(1,128)}), f32[1,64,512]{2,0,1:T(1,128)S(1)}, u32[]{:S(2)}, u32[]{:S(2)}) async-start(f32[1,64,512]{2,0,1:T(1,128)} %broadcast_in_dim_reshape_reshape.4), calls=%async_computation | async-start | bytes 262144 | tf_op jit(solution)/shard_map/all_to_all | solution.py:168
  84.1 37.5 %all-reduce.6.cloned.1.call-start = ((), (), s32[]{:S(2)}) async-start(), calls=%async_computation.4 | async-start | bytes 131072 | tf_op jit(solution)/shard_map/psum | solution.py:204
Sparse Core Ops, SparseCore 0:
  11.0 39.9 all-reduce.3
  104.7 16.7 all-reduce.5
